TPU v7x, 32 devices: a whole 2x2x4 slice. The times are simulated.
32 devices in a mesh: fs: 8 (over z, x), tp: 4 (over y, core).
Axes of the slice: x: 2, y: 2, z: 4, core: 2. Of those that a mesh axis runs over, the one named last changes fastest.
Arguments:
- late_input: bfloat16 [4096, 2048], P(('fs', 'tp')), may hold values from -6 to 6
- norm_gain: bfloat16 [2048], replicated, may hold values from 0.099609375 to 1.8984375
- gate_weight: bfloat16 [2048, 2816], P('fs', 'tp'), may hold values from -0.125 to 0.125
- up_weight: bfloat16 [2048, 2816], P('fs', 'tp'), may hold values from -0.125 to 0.125
- down_weight: bfloat16 [2048, 2816], P('fs', 'tp'), may hold values from -0.109375 to 0.109375
- early_input: bfloat16 [4096, 2048], P(('fs', 'tp')), may hold values from -6 to 6
- cotangent: bfloat16 [4096, 2048], P(('fs', 'tp')), may hold values from -6 to 6
- gate_sum: float32 [2048, 2816], P('fs', 'tp'), may hold values from -192 to 192
- up_sum: float32 [2048, 2816], P('fs', 'tp'), may hold values from -192 to 192
- down_sum: float32 [2048, 2816], P('fs', 'tp'), may hold values from -192 to 192
- gain_sum: float32 [2048], replicated, may hold values from -192 to 192
Outputs:
- late_out: bfloat16 [4096, 2048], P(('fs', 'tp'))
- early_grad: bfloat16 [4096, 2048], P(('fs', 'tp'))
- gate_sum_out: float32 [2048, 2816], P('fs', 'tp')
- up_sum_out: float32 [2048, 2816], P('fs', 'tp')
- down_sum_out: float32 [2048, 2816], P('fs', 'tp')
- gain_sum_out: float32 [2048], replicated
All inputs are finite; a program needn't handle non-finite values.
Results may differ from a plain program's by a relative error of at most 0.008.
Values may be sent and summed in bfloat16 or wider, within the bound.
A program may use at most 128 MiB of HBM per device.

v0:
```python
import jax
import jax.numpy as jnp
from jax import lax
from jax.sharding import PartitionSpec as P

epsilon = 1e-05


def normalize(source, gain_f):
    values = source.astype(jnp.float32)
    scale = lax.rsqrt(jnp.mean(values * values, axis=-1, keepdims=True) + epsilon)
    return ((values * scale * gain_f).astype(jnp.bfloat16), scale, values)


def times_transposed(left, right):
    return lax.dot_general(
        left, right, (((1,), (1,)), ((), ())), preferred_element_type=jnp.float32
    )


def column_product(left, right):
    return lax.dot_general(
        left, right, (((0,), (0,)), ((), ())), preferred_element_type=jnp.float32
    )


def per_device(
    late_input,
    norm_gain,
    gate_weight,
    up_weight,
    down_weight,
    early_input,
    cotangent,
    gate_sum,
    up_sum,
    down_sum,
    gain_sum,
):
    gate_whole, up_whole, down_whole = (
        lax.all_gather(gate_weight, "fs", axis=0, tiled=True),
        lax.all_gather(up_weight, "fs", axis=0, tiled=True),
        lax.all_gather(down_weight, "fs", axis=0, tiled=True),
    )
    gain_f = norm_gain.astype(jnp.float32)
    width = gate_weight.shape[1]
    normed, scale, values = normalize(late_input, gain_f)
    piece = lax.all_gather(normed, "tp", axis=0, tiled=True)
    gate = jnp.dot(piece, gate_whole, preferred_element_type=jnp.float32)
    upper = jnp.dot(piece, up_whole, preferred_element_type=jnp.float32)
    hidden = (jax.nn.silu(gate) * upper).astype(jnp.bfloat16)
    mixed = lax.psum_scatter(
        times_transposed(hidden, down_whole).astype(jnp.bfloat16),
        "tp",
        scatter_dimension=0,
        tiled=True,
    ).astype(jnp.float32)
    late_out = (values + 0.5 * mixed).astype(jnp.bfloat16)
    normed_e, scale_e, values_e = normalize(early_input, gain_f)
    normed_all = lax.all_gather(normed_e, "tp", axis=0, tiled=True)
    cot_all = lax.all_gather(cotangent, "tp", axis=0, tiled=True)
    gate_e = jnp.dot(normed_all, gate_whole, preferred_element_type=jnp.float32)
    upper_e = jnp.dot(normed_all, up_whole, preferred_element_type=jnp.float32)
    sigma_e = jax.nn.sigmoid(gate_e)
    hidden_e = (gate_e * sigma_e * upper_e).astype(jnp.bfloat16)
    d_hidden = 0.5 * jnp.dot(cot_all, down_whole, preferred_element_type=jnp.float32)
    d_gate = (d_hidden * upper_e * sigma_e * (1.0 + gate_e * (1.0 - sigma_e))).astype(jnp.bfloat16)
    d_up = (d_hidden * gate_e * sigma_e).astype(jnp.bfloat16)
    d_normed = lax.psum_scatter(
        (times_transposed(d_gate, gate_whole) + times_transposed(d_up, up_whole)).astype(
            jnp.bfloat16
        ),
        "tp",
        scatter_dimension=0,
        tiled=True,
    ).astype(jnp.float32)
    scaled_grad = d_normed * gain_f
    early_grad = (
        cotangent.astype(jnp.float32)
        + scale_e * scaled_grad
        - values_e * scale_e**3 * jnp.mean(values_e * scaled_grad, axis=-1, keepdims=True)
    ).astype(jnp.bfloat16)
    gain_part = jnp.sum(d_normed * values_e * scale_e, axis=0)
    gain_sum_out = gain_sum + lax.psum(gain_part, ("fs", "tp"))
    summed = lax.psum_scatter(
        jnp.concatenate(
            [
                column_product(normed_all, d_gate),
                column_product(normed_all, d_up),
                0.5 * column_product(cot_all, hidden_e),
            ],
            axis=1,
        ),
        "fs",
        scatter_dimension=0,
        tiled=True,
    )
    gate_grad = summed[:, :width]
    up_grad = summed[:, width : 2 * width]
    down_grad = summed[:, 2 * width :]
    early_grad, gate_sum_out, up_sum_out, down_sum_out, gain_sum_out = (
        early_grad,
        gate_sum + gate_grad,
        up_sum + up_grad,
        down_sum + down_grad,
        gain_sum_out,
    )
    return (late_out, early_grad, gate_sum_out, up_sum_out, down_sum_out, gain_sum_out)


def solution(mesh):
    placed = (
        P(("fs", "tp"), None),
        P(),
        P("fs", "tp"),
        P("fs", "tp"),
        P("fs", "tp"),
        P(("fs", "tp"), None),
        P(("fs", "tp"), None),
        P("fs", "tp"),
        P("fs", "tp"),
        P("fs", "tp"),
        P(),
    )
    return jax.shard_map(
        per_device,
        mesh=mesh,
        in_specs=placed,
        out_specs=(
            P(("fs", "tp"), None),
            P(("fs", "tp"), None),
            P("fs", "tp"),
            P("fs", "tp"),
            P("fs", "tp"),
            P(),
        ),
        check_vma=False,
    )
```

profile of v0, /device:TPU:0, one launch (start us, length us, event | category | flops | bytes accessed | tf_op | source)
XLA Modules:
  0.0 657.0 jit_solution(9303688887401447348)
XLA Ops:
  7.2 1.2 fusion.9
  8.5 0.7 convert_element_type.49
  9.1 2.0 fusion.11
  11.2 0.7 all-gather.9.cloned.1.call-update
  12.0 0.7 all-gather.11.cloned.1.call-update
  13.9 22.7 %all-gather.17.cloned.1.call-done = bf16[512,2048]{1,0:T(8,128)(2,1)} async-done(((bf16[128,2048]{1,0:T(8,128)(2,1)}), bf16[512,2048]{1,0:T(8,128)(2,1)}) %all-gather.17.cloned.1.call-update) | async-done | bytes 2097168 | tf_op jit(solution)/shard_map/all_gather | solution.py:60
  36.6 61.6 %all-gather.9.cloned.1.call-done = bf16[2048,704]{0,1:T(8,128)(2,1)} async-done(((bf16[256,704]{0,1:T(8,128)(2,1)}), bf16[2048,704]{0,1:T(8,128)(2,1)}) %all-gather.9.cloned.1.call-update) | async-done | bytes 2883600 | tf_op jit(solution)/shard_map/all_gather | solution.py:41
  98.3 5.2 fusion.21
  103.5 54.6 %all-gather.11.cloned.1.call-done = bf16[2048,704]{0,1:T(8,128)(2,1)} async-done(((bf16[256,704]{0,1:T(8,128)(2,1)}), bf16[2048,704]{0,1:T(8,128)(2,1)}) %all-gather.11.cloned.1.call-update) | async-done | bytes 2883600 | tf_op jit(solution)/shard_map/all_gather | solution.py:42
  158.1 4.6 fusion.20
  162.7 17.6 %all-gather.15.cloned.1.call-done = bf16[512,2048]{1,0:T(8,128)(2,1)} async-done(((bf16[128,2048]{1,0:T(8,128)(2,1)}), bf16[512,2048]{1,0:T(8,128)(2,1)}) %all-gather.15.cloned.1.call-update) | async-done | bytes 2097168 | tf_op jit(solution)/shard_map/all_gather | solution.py:61
  180.3 61.5 %all-gather.13.cloned.1.call-done = bf16[2048,704]{0,1:T(8,128)(2,1)} async-done(((bf16[256,704]{0,1:T(8,128)(2,1)}), bf16[2048,704]{0,1:T(8,128)(2,1)}) %all-gather.13.cloned.1.call-update) | async-done | bytes 2883600 | tf_op jit(solution)/shard_map/all_gather | solution.py:43
  241.8 5.5 multiply_convert_fusion.1
  247.4 1.8 fusion.22
  249.7 3.4 add_convert_fusion
  253.1 1.0 copy-done.2
  254.3 28.3 %reduce-scatter.6.cloned.1.call-done = bf16[128,2048]{1,0:T(8,128)(2,1)} async-done(((bf16[512,2048]{1,0:T(8,128)(2,1)}), bf16[128,2048]{1,0:T(8,128)(2,1)}) %reduce-scatter.6.cloned.1.call-update) | async-done | bytes 524304 | tf_op jit(solution)/shard_map/reduce_scatter | solution.py:69
  282.6 1.4 fusion.15
  284.0 2.7 fusion.4
  286.9 22.5 %all-gather.7.cloned.1.call-done = bf16[512,2048]{1,0:T(8,128)(2,1)} async-done(((bf16[128,2048]{1,0:T(8,128)(2,1)}), bf16[512,2048]{1,0:T(8,128)(2,1)}) %all-gather.7.cloned.1.call-update) | async-done | bytes 2097168 | tf_op jit(solution)/shard_map/all_gather | solution.py:48
  309.4 5.2 fusion.19
  314.6 8.6 %convolution_convert_fusion = bf16[512,2048]{1,0:T(8,128)(2,1)} fusion(bf16[2048,704]{0,1:T(8,128)(2,1)} %all-gather.13.cloned.1.call-done, bf16[512,2048]{1,0:T(8,128)(2,1)} %all-gather.7.cloned.1.call-done, bf16[2048,704]{0,1:T(8,128)(2,1)} %all-gather.11.cloned.1.call-done, f32[512,704]{0,1:T(8,128)} %fusion.19), kind=kOutput, calls=%fused_computation.3 | convolution fusion | flops 2956001280 | bytes 11403264 | tf_op jit(solution)/shard_map/dot_general | solution.py:16
  323.3 1.0 copy-done.7
  324.3 1.7 fusion.24
  326.0 1.7 fusion.23
  328.4 1.7 multiply_bitcast_fusion
  330.1 6.6 pad_maximum_fusion
  336.7 40.6 %psum.7 = f32[2048]{0:T(1024)S(1)} all-reduce(f32[2048]{0:T(1024)S(1)} %get-tuple-element.6), channel_id=1, replica_groups=mesh['fs'=8,'tp'=4] {'fs','tp'}, use_global_device_ids=true, to_apply=%region_7.8 | all-reduce | flops 2048 | bytes 16384 | tf_op jit(solution)/shard_map/psum | solution.py:84
  377.3 0.6 add.69
  377.9 2.0 fusion.8
  379.9 267.6 %reduce-scatter.8.cloned.1.call-done = f32[256,2112]{0,1:T(8,128)} async-done(((f32[2048,2112]{0,1:T(8,128)}), f32[256,2112]{0,1:T(8,128)}) %reduce-scatter.8.cloned.1.call-update) | async-done | bytes 2162704 | tf_op jit(solution)/shard_map/reduce_scatter | solution.py:85
  647.5 3.0 slice_add_fusion
  (51 shorter events, 3.1 us)
Async XLA Ops:
  7.2 29.5 %all-gather.17.cloned.1.call-start = ((), (), s32[]{:S(2)}) async-start(), calls=%async_computation.9 | async-start | bytes 2621440 | tf_op jit(solution)/shard_map/all_gather | solution.py:60
  11.2 87.1 %all-gather.9.cloned.1.call-start = ((), (), s32[]{:S(2)}) async-start(), calls=%async_computation.4 | async-start | bytes 3244032 | tf_op jit(solution)/shard_map/all_gather | solution.py:41
  11.9 146.1 %all-gather.11.cloned.1.call-start = ((), (), s32[]{:S(2)}) async-start(), calls=%async_computation.5 | async-start | bytes 3244032 | tf_op jit(solution)/shard_map/all_gather | solution.py:42
  12.7 167.6 %all-gather.15.cloned.1.call-start = ((), (), s32[]{:S(2)}) async-start(), calls=%async_computation.8 | async-start | bytes 2621440 | tf_op jit(solution)/shard_map/all_gather | solution.py:61
  13.3 228.5 %all-gather.13.cloned.1.call-start = ((), (), s32[]{:S(2)}) async-start(), calls=%async_computation.6 | async-start | bytes 3244032 | tf_op jit(solution)/shard_map/all_gather | solution.py:43
  13.8 268.8 %reduce-scatter.6.cloned.1.call-start = ((), (), s32[]{:S(2)}) async-start(), calls=%async_computation.10 | async-start | bytes 2621440 | tf_op jit(solution)/shard_map/reduce_scatter | solution.py:69
  36.6 121.5 %copy-start.1 = (bf16[512,2048]{1,0:T(8,128)(2,1)S(1)}, bf16[512,2048]{1,0:T(8,128)(2,1)}, u32[]{:S(2)}) copy-start(bf16[512,2048]{1,0:T(8,128)(2,1)} %all-gather.17.cloned.1.call-done) | copy-start | bytes 6291460
  241.8 5.6 copy-start.5
  247.3 1.9 copy-start.3
  247.3 1.9 copy-start.6
  247.4 2.3 copy-start.12
  253.1 1.0 copy-start.2
  253.1 29.5 %copy-start = (bf16[128,2048]{1,0:T(8,128)(2,1)S(1)}, bf16[128,2048]{1,0:T(8,128)(2,1)}, u32[]{:S(2)}) copy-start(bf16[128,2048]{1,0:T(8,128)(2,1)} %param.16) | copy-start | bytes 1572868
  253.1 56.3 %all-gather.7.cloned.1.call-start = ((), (), s32[]{:S(2)}) async-start(), calls=%async_computation.3 | async-start | bytes 2621440 | tf_op jit(solution)/shard_map/all_gather | solution.py:48
  286.7 91.2 %reduce-scatter.4.cloned.1.call-start = ((), (), s32[]{:S(2)}) async-start(), calls=%async_computation.7 | async-start | bytes 2621440 | tf_op jit(solution)/shard_map/reduce_scatter | solution.py:52
  323.2 1.1 copy-start.7
  323.2 324.3 %reduce-scatter.8.cloned.1.call-start = ((), (), s32[]{:S(2)}) async-start(), calls=%async_computation.11 | async-start | bytes 19464192 | tf_op jit(solution)/shard_map/reduce_scatter | solution.py:85
  324.3 1.7 copy-start.4
  326.0 1.7 copy-start.13
  326.0 2.0 copy-start.14
  326.0 2.4 copy-start.15
  336.7 40.6 %copy-start.11 = (f32[2048]{0:T(1024)S(1)}, f32[2048]{0:T(1024)}, u32[]{:S(2)}) copy-start(f32[2048]{0:T(1024)} %param.21) | copy-start | bytes 24580
  336.7 310.8 %copy-start.10 = (f32[256,704]{0,1:T(8,128)S(1)}, f32[256,704]{0,1:T(8,128)}, u32[]{:S(2)}) copy-start(f32[256,704]{0,1:T(8,128)} %param.18) | copy-start | bytes 2162692
  336.7 310.8 %copy-start.8 = (f32[256,704]{0,1:T(8,128)S(1)}, f32[256,704]{0,1:T(8,128)}, u32[]{:S(2)}) copy-start(f32[256,704]{0,1:T(8,128)} %param.20) | copy-start | bytes 2162692
  336.7 310.8 %copy-start.9 = (f32[256,704]{0,1:T(8,128)S(1)}, f32[256,704]{0,1:T(8,128)}, u32[]{:S(2)}) copy-start(f32[256,704]{0,1:T(8,128)} %param.19) | copy-start | bytes 2162692
Sparse Core Ops, SparseCore 0:
  11.3 25.2 all-gather.16
  38.7 59.5 all-gather.8
  100.3 57.7 all-gather.10
  159.5 20.7 all-gather.14
  182.2 59.5 all-gather.12
  253.2 29.3 reduce-scatter.5
  286.8 22.5 all-gather.6
  323.3 31.8 reduce-scatter.3
  359.2 288.2 reduce-scatter.7
where the time goes:
time: 658 us; the launch traced here: 657 us
  waiting for transfers between devices  539 us (82%)
  blocking collectives  40.6 us (6%)
  matrix products  39.4 us (6%)
  other arithmetic  20.3 us (3%)
  between operations  14 us (2%)
    reduce_scatter x1, waiting for transfers between devices, per_device(): lax.psum_scatter(jnp.concatenate([column_product(normed_all, d_gate), col...  268 us
    all_gather x1, waiting for transfers between devices, per_device(): lax.all_gather(gate_weight, 'fs', axis=0, tiled=True)  61.6 us
    all_gather x1, waiting for transfers between devices, per_device(): lax.all_gather(down_weight, 'fs', axis=0, tiled=True)  61.5 us
    all_gather x1, waiting for transfers between devices, per_device(): lax.all_gather(up_weight, 'fs', axis=0, tiled=True)  54.6 us
    psum x1, blocking collectives, per_device(): gain_sum_out = gain_sum + lax.psum(gain_part, ('fs', 'tp'))  40.6 us
    reduce_scatter x1, waiting for transfers between devices, per_device(): lax.psum_scatter((times_transposed(d_gate, gate_whole) + times_transposed...  28.3 us
    all_gather x1, waiting for transfers between devices, per_device(): normed_all = lax.all_gather(normed_e, 'tp', axis=0, tiled=True)  22.7 us
    all_gather x1, waiting for transfers between devices, per_device(): piece = lax.all_gather(normed, 'tp', axis=0, tiled=True)  22.5 us
  transfers between devices with their start and end apart: 9, of which 8 were waited for; matrix products, arithmetic and copies ran while one was open for 4% of the time, Pallas kernels for 0%

commit v1 on v0

--- a/solution.py
+++ b/solution.py
@@ -81,7 +81,7 @@
         - values_e * scale_e**3 * jnp.mean(values_e * scaled_grad, axis=-1, keepdims=True)
     ).astype(jnp.bfloat16)
     gain_part = jnp.sum(d_normed * values_e * scale_e, axis=0)
-    gain_sum_out = gain_sum + lax.psum(gain_part, ("fs", "tp"))
+    gain_sum_out = gain_sum + lax.psum(lax.psum(gain_part, "tp"), "fs")
     summed = lax.psum_scatter(
         jnp.concatenate(
             [

time: 658 us -> 657 us (level)
  blocking collectives: 40.6 us -> 27.9 us
  waiting for transfers between devices: 539 us -> 550 us
    psum x1 -> x2, blocking collectives: 40.6 us -> 27.9 us  [per_device(): gain_sum_out = gain_sum + lax.psum(lax.psum(gain_part, 'tp'), 'fs')]
    reduce_scatter x1, waiting for transfers between devices: 268 us -> 279 us  [per_device(): lax.psum_scatter(jnp.concatenate([column_product(normed_all, d_gate), col...]
where the time goes in v1:
time: 657 us; the launch traced here: 656 us
  waiting for transfers between devices  550 us (84%)
  matrix products  39.4 us (6%)
  blocking collectives  27.9 us (4%)
  other arithmetic  20.5 us (3%)
  between operations  14 us (2%)
    reduce_scatter x1, waiting for transfers between devices, per_device(): lax.psum_scatter(jnp.concatenate([column_product(normed_all, d_gate), col...  279 us
    all_gather x1, waiting for transfers between devices, per_device(): lax.all_gather(gate_weight, 'fs', axis=0, tiled=True)  61.6 us
    all_gather x1, waiting for transfers between devices, per_device(): lax.all_gather(down_weight, 'fs', axis=0, tiled=True)  61.5 us
    all_gather x1, waiting for transfers between devices, per_device(): lax.all_gather(up_weight, 'fs', axis=0, tiled=True)  54.6 us
    reduce_scatter x1, waiting for transfers between devices, per_device(): lax.psum_scatter((times_transposed(d_gate, gate_whole) + times_transposed...  28.3 us
    psum x2, blocking collectives, per_device(): gain_sum_out = gain_sum + lax.psum(lax.psum(gain_part, 'tp'), 'fs')  27.9 us
    all_gather x1, waiting for transfers between devices, per_device(): normed_all = lax.all_gather(normed_e, 'tp', axis=0, tiled=True)  22.7 us
    all_gather x1, waiting for transfers between devices, per_device(): piece = lax.all_gather(normed, 'tp', axis=0, tiled=True)  22.5 us
  transfers between devices with their start and end apart: 9, of which 8 were waited for; matrix products, arithmetic and copies ran while one was open for 4% of the time, Pallas kernels for 0%

profile of v1, /device:TPU:0, one launch (start us, length us, event | category | flops | bytes accessed | tf_op | source)
XLA Modules:
  0.0 655.9 jit_solution(357755541682923632)
XLA Ops:
  7.2 1.2 fusion.9
  8.5 0.7 convert_element_type.49
  9.1 2.0 fusion.11
  11.2 0.7 all-gather.9.cloned.1.call-update
  12.0 0.7 all-gather.11.cloned.1.call-update
  13.9 22.7 %all-gather.17.cloned.1.call-done = bf16[512,2048]{1,0:T(8,128)(2,1)} async-done(((bf16[128,2048]{1,0:T(8,128)(2,1)}), bf16[512,2048]{1,0:T(8,128)(2,1)}) %all-gather.17.cloned.1.call-update) | async-done | bytes 2097168 | tf_op jit(solution)/shard_map/all_gather | solution.py:60
  36.6 61.6 %all-gather.9.cloned.1.call-done = bf16[2048,704]{0,1:T(8,128)(2,1)} async-done(((bf16[256,704]{0,1:T(8,128)(2,1)}), bf16[2048,704]{0,1:T(8,128)(2,1)}) %all-gather.9.cloned.1.call-update) | async-done | bytes 2883600 | tf_op jit(solution)/shard_map/all_gather | solution.py:41
  98.3 5.2 fusion.21
  103.5 54.6 %all-gather.11.cloned.1.call-done = bf16[2048,704]{0,1:T(8,128)(2,1)} async-done(((bf16[256,704]{0,1:T(8,128)(2,1)}), bf16[2048,704]{0,1:T(8,128)(2,1)}) %all-gather.11.cloned.1.call-update) | async-done | bytes 2883600 | tf_op jit(solution)/shard_map/all_gather | solution.py:42
  158.1 4.6 fusion.20
  162.7 17.6 %all-gather.15.cloned.1.call-done = bf16[512,2048]{1,0:T(8,128)(2,1)} async-done(((bf16[128,2048]{1,0:T(8,128)(2,1)}), bf16[512,2048]{1,0:T(8,128)(2,1)}) %all-gather.15.cloned.1.call-update) | async-done | bytes 2097168 | tf_op jit(solution)/shard_map/all_gather | solution.py:61
  180.3 61.5 %all-gather.13.cloned.1.call-done = bf16[2048,704]{0,1:T(8,128)(2,1)} async-done(((bf16[256,704]{0,1:T(8,128)(2,1)}), bf16[2048,704]{0,1:T(8,128)(2,1)}) %all-gather.13.cloned.1.call-update) | async-done | bytes 2883600 | tf_op jit(solution)/shard_map/all_gather | solution.py:43
  241.8 5.5 multiply_convert_fusion.1
  247.4 1.8 fusion.22
  249.7 3.4 add_convert_fusion
  253.1 1.0 copy-done.2
  254.3 28.3 %reduce-scatter.6.cloned.1.call-done = bf16[128,2048]{1,0:T(8,128)(2,1)} async-done(((bf16[512,2048]{1,0:T(8,128)(2,1)}), bf16[128,2048]{1,0:T(8,128)(2,1)}) %reduce-scatter.6.cloned.1.call-update) | async-done | bytes 524304 | tf_op jit(solution)/shard_map/reduce_scatter | solution.py:69
  282.6 1.4 fusion.15
  284.0 2.7 fusion.4
  286.9 22.5 %all-gather.7.cloned.1.call-done = bf16[512,2048]{1,0:T(8,128)(2,1)} async-done(((bf16[128,2048]{1,0:T(8,128)(2,1)}), bf16[512,2048]{1,0:T(8,128)(2,1)}) %all-gather.7.cloned.1.call-update) | async-done | bytes 2097168 | tf_op jit(solution)/shard_map/all_gather | solution.py:48
  309.4 5.2 fusion.19
  314.6 8.5 %convolution_convert_fusion = bf16[512,2048]{1,0:T(8,128)(2,1)} fusion(bf16[2048,704]{0,1:T(8,128)(2,1)} %all-gather.13.cloned.1.call-done, bf16[512,2048]{1,0:T(8,128)(2,1)} %all-gather.7.cloned.1.call-done, bf16[2048,704]{0,1:T(8,128)(2,1)} %all-gather.11.cloned.1.call-done, f32[512,704]{0,1:T(8,128)} %fusion.19), kind=kOutput, calls=%fused_computation.3 | convolution fusion | flops 2956001280 | bytes 11403264 | tf_op jit(solution)/shard_map/dot_general | solution.py:16
  323.2 1.0 copy-done.7
  324.3 1.7 fusion.24
  326.0 1.7 fusion.23
  328.4 1.7 multiply_bitcast_fusion
  330.1 6.6 pad_maximum_fusion
  336.7 6.1 psum.14
  342.8 21.8 %psum.15 = f32[2048]{0:T(1024)S(1)} all-reduce(f32[2048]{0:T(1024)S(1)} %psum.14), channel_id=1, replica_groups=mesh['fs'=8,'tp'=4] {'fs'}, use_global_device_ids=true, to_apply=%region_8.9 | all-reduce | flops 2048 | bytes 16384 | tf_op jit(solution)/shard_map/psum | solution.py:84
  365.2 2.1 fusion.8
  367.4 279.0 %reduce-scatter.8.cloned.1.call-done = f32[256,2112]{0,1:T(8,128)} async-done(((f32[2048,2112]{0,1:T(8,128)}), f32[256,2112]{0,1:T(8,128)}) %reduce-scatter.8.cloned.1.call-update) | async-done | bytes 2162704 | tf_op jit(solution)/shard_map/reduce_scatter | solution.py:85
  646.4 3.0 slice_add_fusion
  (52 shorter events, 3.7 us)
Async XLA Ops:
  7.2 29.5 %all-gather.17.cloned.1.call-start = ((), (), s32[]{:S(2)}) async-start(), calls=%async_computation.9 | async-start | bytes 2621440 | tf_op jit(solution)/shard_map/all_gather | solution.py:60
  11.2 87.1 %all-gather.9.cloned.1.call-start = ((), (), s32[]{:S(2)}) async-start(), calls=%async_computation.4 | async-start | bytes 3244032 | tf_op jit(solution)/shard_map/all_gather | solution.py:41
  11.9 146.1 %all-gather.11.cloned.1.call-start = ((), (), s32[]{:S(2)}) async-start(), calls=%async_computation.5 | async-start | bytes 3244032 | tf_op jit(solution)/shard_map/all_gather | solution.py:42
  12.7 167.6 %all-gather.15.cloned.1.call-start = ((), (), s32[]{:S(2)}) async-start(), calls=%async_computation.8 | async-start | bytes 2621440 | tf_op jit(solution)/shard_map/all_gather | solution.py:61
  13.3 228.5 %all-gather.13.cloned.1.call-start = ((), (), s32[]{:S(2)}) async-start(), calls=%async_computation.6 | async-start | bytes 3244032 | tf_op jit(solution)/shard_map/all_gather | solution.py:43
  13.8 268.7 %reduce-scatter.6.cloned.1.call-start = ((), (), s32[]{:S(2)}) async-start(), calls=%async_computation.10 | async-start | bytes 2621440 | tf_op jit(solution)/shard_map/reduce_scatter | solution.py:69
  36.6 121.5 %copy-start.1 = (bf16[512,2048]{1,0:T(8,128)(2,1)S(1)}, bf16[512,2048]{1,0:T(8,128)(2,1)}, u32[]{:S(2)}) copy-start(bf16[512,2048]{1,0:T(8,128)(2,1)} %all-gather.17.cloned.1.call-done) | copy-start | bytes 6291460
  241.8 5.6 copy-start.5
  247.3 1.9 copy-start.3
  247.3 1.9 copy-start.6
  247.4 2.3 copy-start.12
  253.0 1.0 copy-start.2
  253.0 29.5 %copy-start = (bf16[128,2048]{1,0:T(8,128)(2,1)S(1)}, bf16[128,2048]{1,0:T(8,128)(2,1)}, u32[]{:S(2)}) copy-start(bf16[128,2048]{1,0:T(8,128)(2,1)} %param.16) | copy-start | bytes 1572868
  253.1 56.3 %all-gather.7.cloned.1.call-start = ((), (), s32[]{:S(2)}) async-start(), calls=%async_computation.3 | async-start | bytes 2621440 | tf_op jit(solution)/shard_map/all_gather | solution.py:48
  286.7 78.6 %reduce-scatter.4.cloned.1.call-start = ((), (), s32[]{:S(2)}) async-start(), calls=%async_computation.7 | async-start | bytes 2621440 | tf_op jit(solution)/shard_map/reduce_scatter | solution.py:52
  323.1 1.1 copy-start.7
  323.2 323.2 %reduce-scatter.8.cloned.1.call-start = ((), (), s32[]{:S(2)}) async-start(), calls=%async_computation.11 | async-start | bytes 19464192 | tf_op jit(solution)/shard_map/reduce_scatter | solution.py:85
  324.3 1.7 copy-start.4
  325.9 1.7 copy-start.13
  325.9 2.0 copy-start.14
  325.9 2.4 copy-start.15
  336.6 28.0 %copy-start.11 = (f32[2048]{0:T(1024)S(1)}, f32[2048]{0:T(1024)}, u32[]{:S(2)}) copy-start(f32[2048]{0:T(1024)} %param.21) | copy-start | bytes 24580
  336.6 309.8 %copy-start.10 = (f32[256,704]{0,1:T(8,128)S(1)}, f32[256,704]{0,1:T(8,128)}, u32[]{:S(2)}) copy-start(f32[256,704]{0,1:T(8,128)} %param.18) | copy-start | bytes 2162692
  336.7 309.8 %copy-start.8 = (f32[256,704]{0,1:T(8,128)S(1)}, f32[256,704]{0,1:T(8,128)}, u32[]{:S(2)}) copy-start(f32[256,704]{0,1:T(8,128)} %param.20) | copy-start | bytes 2162692
  336.7 309.8 %copy-start.9 = (f32[256,704]{0,1:T(8,128)S(1)}, f32[256,704]{0,1:T(8,128)}, u32[]{:S(2)}) copy-start(f32[256,704]{0,1:T(8,128)} %param.19) | copy-start | bytes 2162692
Sparse Core Ops, SparseCore 0:
  11.3 25.2 all-gather.16
  38.7 59.5 all-gather.8
  100.3 57.7 all-gather.10
  159.5 20.7 all-gather.14
  182.2 59.5 all-gather.12
  253.2 29.3 reduce-scatter.5
  286.8 22.5 all-gather.6
  323.3 31.2 reduce-scatter.3
  358.5 287.8 reduce-scatter.7
